TPU v7x, 32 devices: a whole 2x2x4 slice. The times are simulated.
32 devices in a mesh: sp: 4 (over z), tp: 2 (over y), dp: 4 (over x, core).
Axes of the slice: x: 2, y: 2, z: 4, core: 2. Of those that a mesh axis runs over, the one named last changes fastest.
Arguments:
- latent: bfloat16 [2048, 2048], P(('dp', 'sp', 'tp')), parts along dimension 0, may hold values from -6 to 6
- cond: bfloat16 [8192], P('dp'), parts along dimension 0, may hold values from -6 to 6
- context: bfloat16 [2048, 2048], P(('dp', 'sp')), parts along dimension 0, may hold values from -6 to 6
- context_cond: bfloat16 [2048], replicated, may hold values from -6 to 6
- modulation: bfloat16 [2048, 6144], P(('sp', 'tp')), may hold values from -0.125 to 0.125
- norm_gain: bfloat16 [2048], replicated, may hold values from 0.099609375 to 1.8984375
- w_x: bfloat16 [2048, 1024], P(None, 'tp'), may hold values from -0.125 to 0.125
- w_gate: bfloat16 [2048, 1024], P(None, 'tp'), may hold values from -0.125 to 0.125
- w_b: bfloat16 [2048, 256], P(None, 'tp'), may hold values from -0.125 to 0.125
- w_c: bfloat16 [2048, 256], P(None, 'tp'), may hold values from -0.125 to 0.125
- w_dt: bfloat16 [2, 2048, 16], P(None, None, 'tp'), may hold values from -0.125 to 0.125
- conv_x: bfloat16 [4, 1024], P(None, 'tp'), may hold values from -3 to 3
- conv_b: bfloat16 [4, 256], P(None, 'tp'), may hold values from -3 to 3
- conv_c: bfloat16 [4, 256], P(None, 'tp'), may hold values from -3 to 3
- decay_rate: float32 [2, 16], P(None, 'tp'), may hold values from 0 to 0.04
- decay_extra: float32 [2048, 16], P(('dp', 'sp'), 'tp'), parts along dimension 0, may hold values from -2 to 0
- out_gain: bfloat16 [1024], P('tp'), may hold values from 0.099609375 to 1.8984375
- w_out: bfloat16 [1024, 2048], replicated, may hold values from -0.1875 to 0.1875
Outputs:
- mixed: bfloat16 [2048, 2048], P(('dp', 'sp', 'tp')), parts along dimension 0
There are 4 independent parts, one for each index of `dp`. A program takes and returns all parts, laid end to end along the dimension named above; an argument that names none is the same for every part. Nothing has to cross between parts.
All inputs are finite; a program needn't handle non-finite values.
Results may differ from a plain program's by a relative error of at most 0.007.
Values may be sent and summed in bfloat16 or wider, within the bound.
A program may use at most 64 MiB of HBM per device.

v0:
```python
import jax
import jax.numpy as jnp
from jax import lax
from jax.sharding import PartitionSpec as P

HEAD_DIM = 64
STATE = 64
BLOCK = 128
ROW_EPS = 1e-06
GROUP_EPS = 1e-05
HIGHEST = lax.Precision.HIGHEST


def prefix(x, axis, join, neutral, backward):
    count = lax.axis_size(axis)
    place = lax.axis_index(axis)
    ahead = count - 1 - place if backward else place
    gathered = jax.tree.map(
        lambda a, kind: lax.all_gather(a.astype(kind), axis),
        x,
        jax.tree.map(lambda a: jnp.bfloat16 if a.dtype == jnp.float32 else a.dtype, x),
    )
    state = jax.tree.map(lambda a, e: jnp.zeros_like(a) + jnp.asarray(e, a.dtype), x, neutral)

    def one(hop, state):
        source = count - 1 - hop if backward else hop
        return join(
            state,
            jax.tree.map(
                lambda a, own: lax.dynamic_index_in_dim(a, source, 0, False).astype(own.dtype),
                gathered,
                x,
            ),
        )

    return lax.fori_loop(0, ahead, one, state)


def with_halo(block, sides, width):
    for axis, dim in sides:
        count = lax.axis_size(axis)
        forward = [(i, i + 1) for i in range(count - 1)]
        backward = [(target, source) for source, target in forward]
        low = lax.ppermute(
            lax.slice_in_dim(block, block.shape[dim] - width, None, axis=dim), axis, forward
        )
        high = lax.ppermute(lax.slice_in_dim(block, 0, width, axis=dim), axis, backward)
        block = jnp.concatenate([low, block, high], axis=dim)
    return block


def modulated_norm(row_block, norm_gain, shift_row, scale_row):
    values = row_block.astype(jnp.float32)
    normed = values * lax.rsqrt(jnp.mean(values * values, axis=-1, keepdims=True) + ROW_EPS)
    return (normed * norm_gain.astype(jnp.float32) * (1.0 + scale_row) + shift_row).astype(
        jnp.bfloat16
    )


def project_many(row_block, weights):
    return jnp.concatenate(
        [
            jnp.dot(row_block, weight, preferred_element_type=jnp.float32).astype(jnp.bfloat16)
            for weight in weights
        ],
        axis=1,
    )


def conv_padded(padded, conv_taps, length):
    values = padded.astype(jnp.float32)
    summed = jnp.zeros((length, values.shape[1]), jnp.float32)
    for offset in range(conv_taps.shape[0]):
        summed = summed + conv_taps[offset].astype(jnp.float32) * values[offset : offset + length]
    return jax.nn.silu(summed).astype(jnp.bfloat16)


def context_states(ctx_xs, ctx_bmat, ctx_dt, decay_rate):
    length = ctx_xs.shape[0]
    groups = ctx_bmat.shape[1] // STATE
    heads_here = ctx_dt.shape[2]
    repeat = heads_here // groups
    values = ctx_xs.astype(jnp.float32).reshape(length, groups, repeat, HEAD_DIM)
    keys_b = ctx_bmat.astype(jnp.float32).reshape(length, groups, STATE)
    log_decay = -decay_rate[:, None, :] * ctx_dt
    running = jnp.cumsum(log_decay, axis=1)
    forward_weight = (jnp.exp(running[0, -1:] - running[0]) * ctx_dt[0]).reshape(
        length, groups, repeat
    )
    backward_weight = (jnp.exp(running[1] - log_decay[1]) * ctx_dt[1]).reshape(
        length, groups, repeat
    )
    forward_state = jnp.einsum(
        "lgn,lgr,lgrp->grpn", keys_b, forward_weight, values, precision=HIGHEST
    )
    backward_state = jnp.einsum(
        "lgn,lgr,lgrp->grpn", keys_b, backward_weight, values, precision=HIGHEST
    )
    return (forward_state, backward_state)


def block_pass(inputs, step_sizes, log_decay, bmat, cmat, start_state):
    length = inputs.shape[0]
    groups, repeat = (start_state.shape[0], start_state.shape[1])
    block_count = length // BLOCK
    values = inputs.reshape(block_count, BLOCK, groups, repeat, HEAD_DIM)
    steps_blk = step_sizes.reshape(block_count, BLOCK, groups, repeat)
    decays = log_decay.reshape(block_count, BLOCK, groups, repeat)
    keys_b = bmat.reshape(block_count, BLOCK, groups, STATE)
    reads_c = cmat.reshape(block_count, BLOCK, groups, STATE)
    lower_mask = (jnp.arange(BLOCK)[:, None] >= jnp.arange(BLOCK)[None, :])[:, :, None, None]

    def advance(carried, block_data):
        value_blk, step_blk, decay_blk, key_blk, read_blk = block_data
        running = jnp.cumsum(decay_blk, axis=0)
        log_gaps = running[:, None] - running[None, :]
        mixing = jnp.where(lower_mask, jnp.exp(jnp.where(lower_mask, log_gaps, 0.0)), 0.0)
        affinity = jnp.einsum("ign,jgn->ijg", read_blk, key_blk, preferred_element_type=jnp.float32)
        weights = (affinity[..., None] * mixing * step_blk[None]).astype(jnp.bfloat16)
        output = jnp.einsum(
            "ijgr,jgrp->igrp", weights, value_blk, preferred_element_type=jnp.float32
        )
        output = output + jnp.einsum(
            "ign,grpn,igr->igrp",
            read_blk.astype(jnp.float32),
            carried,
            jnp.exp(running),
            precision=HIGHEST,
        )
        to_end = jnp.exp(running[-1:] - running) * step_blk
        state_in = (key_blk.astype(jnp.float32)[:, :, None, :] * to_end[..., None]).astype(
            jnp.bfloat16
        )
        carried = jnp.exp(running[-1])[..., None, None] * carried + jnp.einsum(
            "jgrn,jgrp->grpn", state_in, value_blk, preferred_element_type=jnp.float32
        )
        return (carried, output)

    final_state, outputs = lax.scan(
        advance, start_state, (values, steps_blk, decays, keys_b, reads_c)
    )
    return (outputs.reshape(length, groups, repeat, HEAD_DIM), final_state)


def state_chain(summary, backward):

    def combine(earlier, later_part):
        return (
            earlier[0] + later_part[0],
            jnp.exp(later_part[0])[..., None, None] * earlier[1] + later_part[1],
        )

    identity_pair = (jnp.zeros_like(summary[0]), jnp.zeros_like(summary[1]))
    return prefix(summary, "sp", combine, identity_pair, backward)


def directed_pass(inputs, step_sizes, log_decay, bmat, cmat, outer_start, zeros_state, backward):
    local_out, final_state = block_pass(inputs, step_sizes, log_decay, bmat, cmat, zeros_state)
    length = inputs.shape[0]
    groups, repeat = (zeros_state.shape[0], zeros_state.shape[1])
    running = jnp.cumsum(log_decay, axis=0).reshape(length, groups, repeat)
    before = state_chain((running[-1], final_state), backward)
    entry_state = jnp.exp(before[0])[..., None, None] * outer_start + before[1]
    read_rows = cmat.astype(jnp.float32).reshape(length, groups, STATE)
    return local_out + jnp.einsum(
        "tgn,grpn,tgr->tgrp", read_rows, entry_state, jnp.exp(running), precision=HIGHEST
    )


def group_norm(combined, out_gain):
    length, groups, repeat, _ = combined.shape
    mean_square = jnp.mean(combined * combined, axis=(2, 3), keepdims=True)
    scaled = (
        combined
        * lax.rsqrt(mean_square + GROUP_EPS)
        * out_gain.astype(jnp.float32).reshape(groups, repeat, HEAD_DIM)
    )
    return scaled.reshape(length, groups * repeat * HEAD_DIM).astype(jnp.bfloat16)


def local(
    latent,
    cond,
    context,
    context_cond,
    modulation,
    norm_gain,
    w_x,
    w_gate,
    w_b,
    w_c,
    w_dt,
    conv_x,
    conv_b,
    conv_c,
    decay_rate,
    decay_extra,
    out_gain,
    w_out,
):
    model_width = latent.shape[1]
    mod_share = modulation.shape[0]
    cond_rows = jax.nn.silu(jnp.stack([cond, context_cond]).astype(jnp.float32)).astype(
        jnp.bfloat16
    )
    own_cols = lax.dynamic_slice_in_dim(
        cond_rows, lax.axis_index(("sp", "tp")) * mod_share, mod_share, 1
    )
    mod_rows = lax.psum(
        jnp.dot(own_cols, modulation, preferred_element_type=jnp.float32), ("sp", "tp")
    )
    shift_rows = mod_rows[:, :model_width]
    scale_rows = mod_rows[:, model_width : 2 * model_width]
    gate_row = mod_rows[0, 2 * model_width :]
    head_cols = w_x.shape[1]
    state_cols = w_b.shape[1]
    heads_here = w_dt.shape[2]
    groups_here = state_cols // STATE
    repeat = heads_here // groups_here
    hidden = modulated_norm(latent, norm_gain, shift_rows[0], scale_rows[0])
    latent_mats = (w_x, w_b, w_c, w_gate, w_dt[0], w_dt[1])
    projected = project_many(lax.all_gather(hidden, "tp", axis=0, tiled=True), latent_mats)
    token_count = projected.shape[0]
    conv_cols = head_cols + 2 * state_cols
    extended = with_halo(projected[:, :conv_cols], (("sp", 0),), 2)
    conv_taps = jnp.concatenate([conv_x, conv_b, conv_c], axis=1)
    convolved = conv_padded(extended, conv_taps, token_count)
    latent_xs = convolved[:, :head_cols]
    latent_b = convolved[:, head_cols : head_cols + state_cols]
    latent_c = convolved[:, head_cols + state_cols :]
    gate_in = projected[:, conv_cols : conv_cols + head_cols]
    dt_start = conv_cols + head_cols
    latent_dt = jnp.stack(
        [
            jax.nn.softplus(projected[:, dt_start : dt_start + heads_here].astype(jnp.float32)),
            jax.nn.softplus(projected[:, dt_start + heads_here :].astype(jnp.float32)),
        ]
    )
    context_mats = (w_x, w_b, w_dt[0], w_dt[1])
    own_context = project_many(
        modulated_norm(context, norm_gain, shift_rows[1], scale_rows[1]), context_mats
    )
    context_cols = lax.all_gather(own_context, "sp", axis=0, tiled=True)
    ctx_span = head_cols + state_cols
    ctx_padded = jnp.pad(context_cols[:, :ctx_span], ((2, 1), (0, 0)))
    ctx_conv = conv_padded(
        ctx_padded, jnp.concatenate([conv_x, conv_b], axis=1), context_cols.shape[0]
    )
    ctx_dt = jnp.stack(
        [
            jax.nn.softplus(context_cols[:, ctx_span : ctx_span + heads_here].astype(jnp.float32)),
            jax.nn.softplus(context_cols[:, ctx_span + heads_here :].astype(jnp.float32)),
        ]
    )
    forward_start, backward_start = context_states(
        ctx_conv[:, :head_cols], ctx_conv[:, head_cols:], ctx_dt, decay_rate
    )
    log_decay = -decay_rate[:, None, :] * latent_dt + decay_extra[None]
    zeros_state = jnp.zeros((groups_here, repeat, HEAD_DIM, STATE), jnp.float32)
    y_forward = directed_pass(
        latent_xs, latent_dt[0], log_decay[0], latent_b, latent_c, forward_start, zeros_state, False
    )
    y_backward = directed_pass(
        latent_xs[::-1],
        latent_dt[1][::-1],
        log_decay[1][::-1],
        latent_b[::-1],
        latent_c[::-1],
        backward_start,
        zeros_state,
        True,
    )
    gate_act = jax.nn.silu(gate_in.astype(jnp.float32)).reshape(
        token_count, groups_here, repeat, HEAD_DIM
    )
    combined = (y_forward + y_backward[::-1]) * gate_act
    normed = group_norm(combined, out_gain)
    tp_count = lax.axis_size("tp")
    stacked = normed.reshape(tp_count, token_count // tp_count, normed.shape[1])
    branch = jnp.dot(
        lax.all_to_all(stacked, "tp", split_axis=0, concat_axis=2, tiled=True)[0],
        w_out,
        preferred_element_type=jnp.float32,
    )[None]
    return (latent.astype(jnp.float32) + gate_row * branch[0]).astype(jnp.bfloat16)


def solution(mesh):
    in_specs = (
        P(("dp", "sp", "tp"), None),
        P("dp"),
        P(("dp", "sp"), None),
        P(),
        P(("sp", "tp"), None),
        P(),
        P(None, "tp"),
        P(None, "tp"),
        P(None, "tp"),
        P(None, "tp"),
        P(None, None, "tp"),
        P(None, "tp"),
        P(None, "tp"),
        P(None, "tp"),
        P(None, "tp"),
        P(("dp", "sp"), "tp"),
        P("tp"),
        P(),
    )
    out_specs = P(("dp", "sp", "tp"), None)
    return jax.shard_map(local, mesh=mesh, in_specs=in_specs, out_specs=out_specs, check_vma=False)
```

profile of v0, /device:TPU:0, one launch (start us, length us, event | category | flops | bytes accessed | tf_op | source)
XLA Modules:
  0.0 247.8 jit_solution(15845269503590403432)
XLA Ops:
  2.4 39.4 %psum.7 = f32[2,6144]{1,0:T(2,128)S(1)} all-reduce(f32[2,6144]{1,0:T(2,128)S(1)} %fusion.93), channel_id=1, replica_groups=mesh['sp'=4,'tp'=2,'dp'=4] {'sp','tp'}, use_global_device_ids=true, to_apply=%region_0.1 | all-reduce | flops 12288 | bytes 98304 | tf_op jit(solution)/shard_map/psum | solution.py:209
  42.9 7.2 %all_gather.26 = bf16[128,2048]{1,0:T(8,128)(2,1)S(1)} all-gather(bf16[64,2048]{1,0:T(8,128)(2,1)S(1)} %fusion.31), channel_id=1, replica_groups=mesh['sp'=4,'tp'=2,'dp'=4] {'tp'}, dimensions={0}, use_global_device_ids=true | all-gather | bytes 786432 | tf_op jit(solution)/shard_map/all_gather | solution.py:222
  50.0 2.3 convolution_convert_fusion.2
  53.6 1.9 collective-permute-start
  60.7 2.9 %convolution_convert_fusion.1 = bf16[128,512]{0,1:T(8,128)(2,1)S(1)} fusion(bf16[2048,512]{1,0:T(8,128)(2,1)} %param.28, bf16[128,2048]{1,0:T(8,128)(2,1)} %param.24, f32[2048]{0:T(1024)} %bitcast.249, f32[2048]{0:T(1024)} %bitcast.253, f32[2048]{0:T(1024)S(1)} %convert_element_type.221, f32[128]{0:T(128)S(1)} %add_rsqrt_fusion.1), kind=kOutput, calls=%fused_computation.49 | convolution fusion | flops 270073856 | bytes 2777600 | tf_op jit(solution)/shard_map/dot_general | solution.py:63
  65.2 14.5 %all_gather.30 = bf16[512,656]{0,1:T(8,128)(2,1)S(1)} all-gather(bf16[128,656]{0,1:T(8,128)(2,1)S(1)} %pad_maximum_fusion), channel_id=1, replica_groups=mesh['sp'=4,'tp'=2,'dp'=4] {'sp'}, dimensions={0}, use_global_device_ids=true | all-gather | bytes 839680 | tf_op jit(solution)/shard_map/all_gather | solution.py:243
  93.7 5.0 %reduce-window.6 = f32[2,8,4,128]{3,1,2,0:T(8,128)} reduce-window(f32[2,8,4,128]{3,1,2,0:T(8,128)} %fusion.148, f32[]{:T(128)} %constant.128.clone.1), window={size=1x1x1x128 pad=0_0x0_0x0_0x127_0}, to_apply=%region_7.8 | reduce-window | flops 1040384 | bytes 65540 | tf_op jit(solution)/shard_map/reduce-window
  103.1 2.7 %pad_convert_fusion = f32[515,640]{0,1:T(8,128)} fusion(bf16[512,640]{0,1:T(8,128)(2,1)} %slice.222), kind=kLoop, calls=%fused_computation.67 | loop fusion | flops 329600 | bytes 1973760 | tf_op jit(solution)/shard_map/convert_element_type | solution.py:71
  110.2 3.1 %divide_multiply_fusion = f32[128,512]{1,0:T(8,128)} fusion(bf16[128,2048]{1,0:T(8,128)(2,1)} %copy-done.2, bf16[2048,512]{1,0:T(8,128)(2,1)} %param.29), kind=kOutput, calls=%fused_computation.89 | convolution fusion | flops 268828672 | bytes 2883584 | tf_op jit(solution)/shard_map/dot_general | solution.py:63
  116.3 2.4 multiply_convert_fusion
  118.7 10.4 %all_gather.27 = bf16[4,2,4]{2,1,0:T(2,128)(2,1)} all-gather(bf16[1,2,4]{2,1,0:T(2,128)(2,1)S(1)} %copy-done.55), channel_id=1, replica_groups=mesh['sp'=4,'tp'=2,'dp'=4] {'sp'}, dimensions={0}, use_global_device_ids=true | all-gather | bytes 80 | tf_op jit(solution)/shard_map/all_gather | solution.py:19
  129.1 8.0 %all_gather.31 = bf16[4,2,4]{2,1,0:T(2,128)(2,1)} all-gather(bf16[1,2,4]{2,1,0:T(2,128)(2,1)S(1)} %copy-done.56), channel_id=1, replica_groups=mesh['sp'=4,'tp'=2,'dp'=4] {'sp'}, dimensions={0}, use_global_device_ids=true | all-gather | bytes 80 | tf_op jit(solution)/shard_map/all_gather | solution.py:19
  137.1 1.9 slice.230
  156.2 1.8 copy.190
  164.3 16.6 %all-gather = bf16[8,4,64,64]{3,2,1,0:T(8,128)(2,1)} all-gather(bf16[2,4,64,64]{3,2,1,0:T(8,128)(2,1)S(1)} %fusion.17), channel_id=2, replica_groups=mesh['sp'=4,'tp'=2,'dp'=4] {'sp'}, dimensions={0}, use_global_device_ids=true | all-gather | bytes 327680 | tf_op jit(solution)/shard_map/all_gather | solution.py:19
  182.7 1.6 copy.178
  187.7 19.2 %all-gather.1 = bf16[8,4,64,64]{3,2,1,0:T(8,128)(2,1)} all-gather(bf16[2,4,64,64]{3,2,1,0:T(8,128)(2,1)S(1)} %fusion.18), channel_id=3, replica_groups=mesh['sp'=4,'tp'=2,'dp'=4] {'sp'}, dimensions={0}, use_global_device_ids=true | all-gather | bytes 327680 | tf_op jit(solution)/shard_map/all_gather | solution.py:19
  207.5 7.0 %while.7 = (s32[]{:T(128)}, f32[2,4]{1,0:T(2,128)}, f32[2,4,64,64]{3,2,1,0:T(8,128)S(1)}, s32[]{:T(128)}, bf16[4,2,4]{2,1,0:T(2,128)(2,1)}, /*index=5*/bf16[4,2,...) while((s32[]{:T(128)}, f32[2,4]{1,0:T(2,128)}, f32[2,4,64,64]{3,2,1,0:T(8,128)S(1)}, ...), condition=%wide.region_12.13_spmd, body=%wide.region_11.12_spmd.sunk | while | flops 98326 | bytes 327979 | solution.py:36
  221.6 1.7 fusion.15
  225.5 1.8 rev.23
  229.0 1.7 copy.168
  231.7 1.7 fusion.16
  237.0 6.8 %all_to_all.15 = bf16[2,64,512]{2,1,0:T(8,128)(2,1)S(1)} all-to-all(bf16[2,64,512]{2,1,0:T(8,128)(2,1)S(1)} %copy.199), channel_id=1, replica_groups=mesh['sp'=4,'tp'=2,'dp'=4] {'tp'}, dimensions={0} | all-to-all | bytes 262144 | tf_op jit(solution)/shard_map/all_to_all | solution.py:281
  244.1 3.8 %fusion.1 = bf16[64,2048]{1,0:T(8,128)(2,1)} fusion(bf16[64,1024]{1,0:T(8,128)(2,1)S(1)} %bitcast.213, bf16[1024,2048]{1,0:T(8,128)(2,1)} %param.39, bf16[64,2048]{1,0:T(8,128)(2,1)S(1)} %copy-done.7, f32[2048]{0:T(1024)S(1)} %bitcast.239), kind=kOutput, calls=%fused_computation.10 | convolution fusion | flops 268959744 | bytes 4857856 | tf_op jit(solution)/shard_map/dot_general | solution.py:280
  (238 shorter events, 88.6 us)
Async XLA Ops:
  1.9 40.6 %copy-start.48 = (bf16[2048]{0:T(1024)(128)(2,1)S(1)}, bf16[2048]{0:T(1024)(128)(2,1)}, u32[]{:S(2)}) copy-start(bf16[2048]{0:T(1024)(128)(2,1)} %param.27) | copy-start | bytes 12292
  1.9 40.6 %copy-start.6 = (bf16[64,2048]{1,0:T(8,128)(2,1)S(1)}, bf16[64,2048]{1,0:T(8,128)(2,1)}, u32[]{:S(2)}) copy-start(bf16[64,2048]{1,0:T(8,128)(2,1)} %param.22) | copy-start | bytes 786436
  42.8 9.4 %copy-start.11 = (bf16[2048,128]{1,0:T(8,128)(2,1)S(1)}, bf16[2048,128]{1,0:T(8,128)(2,1)}, u32[]{:S(2)}) copy-start(bf16[2048,128]{1,0:T(8,128)(2,1)} %param.31) | copy-start | bytes 1572868
  50.0 7.0 %copy-start.2 = (bf16[128,2048]{1,0:T(8,128)(2,1)}, bf16[128,2048]{1,0:T(8,128)(2,1)S(1)}, u32[]{:S(2)}) copy-start(bf16[128,2048]{1,0:T(8,128)(2,1)S(1)} %all_gather.26) | copy-start | bytes 1572868
  53.6 105.8 %collective-permute-start = (bf16[2,768]{1,0:T(2,128)(2,1)}, bf16[2,768]{1,0:T(2,128)(2,1)}, u32[]{:S(2)}, u32[]{:S(2)}) collective-permute-start(bf16[2,768]{1,0:T(2,128)(2,1)} %get-tuple-element.220), channel_id=1, source_target_pairs={{0,8},{8,16},{16,24},{1,9},{9,17},{17,25},{2,10},{10,18},{18,26},{... | collective-permute-start | bytes 9224 | tf_op jit(solution)/shard_map/ppermute | solution.py:44
  55.4 103.9 %collective-permute-start.1 = (bf16[2,768]{1,0:T(2,128)(2,1)}, bf16[2,768]{1,0:T(2,128)(2,1)}, u32[]{:S(2)}, u32[]{:S(2)}) collective-permute-start(bf16[2,768]{1,0:T(2,128)(2,1)} %get-tuple-element.221), channel_id=1, source_target_pairs={{8,0},{16,8},{24,16},{9,1},{17,9},{25,17},{10,2},{18,10},{26,18},{... | collective-permute-start | bytes 9224 | tf_op jit(solution)/shard_map/ppermute | solution.py:47
  57.0 29.6 %copy-start.25 = (f32[128,8]{0,1:T(8,128)}, f32[128,8]{0,1:T(8,128)S(1)}, u32[]{:S(2)}) copy-start(f32[128,8]{0,1:T(8,128)S(1)} %compare_select_fusion.3) | copy-start | bytes 12292
  64.8 14.9 %copy-start.37 = (f32[2,8]{1,0:T(2,128)S(1)}, f32[2,8]{1,0:T(2,128)}, u32[]{:S(2)}) copy-start(f32[2,8]{1,0:T(2,128)} %copy-done.36) | copy-start | bytes 196
  65.2 17.6 %copy-start.41 = (f32[128,8]{0,1:T(8,128)S(1)}, f32[128,8]{0,1:T(8,128)}, u32[]{:S(2)}) copy-start(f32[128,8]{0,1:T(8,128)} %get-tuple-element.233) | copy-start | bytes 12292
  65.2 24.9 %copy-start.38 = (f32[128,8]{0,1:T(8,128)S(1)}, f32[128,8]{0,1:T(8,128)}, u32[]{:S(2)}) copy-start(f32[128,8]{0,1:T(8,128)} %get-tuple-element.232) | copy-start | bytes 12292
  110.2 6.1 %copy-start.1 = (f32[515,640]{0,1:T(8,128)S(1)}, f32[515,640]{0,1:T(8,128)}, u32[]{:S(2)}) copy-start(f32[515,640]{0,1:T(8,128)} %pad_convert_fusion) | copy-start | bytes 3955204
  110.2 6.1 %copy-start.42 = (f32[640]{0:T(1024)S(1)}, f32[640]{0:T(1024)}, u32[]{:S(2)}) copy-start(f32[640]{0:T(1024)} %get-tuple-element.183) | copy-start | bytes 7684
  110.2 6.1 %copy-start.43 = (f32[640]{0:T(1024)S(1)}, f32[640]{0:T(1024)}, u32[]{:S(2)}) copy-start(f32[640]{0:T(1024)} %get-tuple-element.184) | copy-start | bytes 7684
  110.2 6.1 %copy-start.44 = (f32[640]{0:T(1024)S(1)}, f32[640]{0:T(1024)}, u32[]{:S(2)}) copy-start(f32[640]{0:T(1024)} %get-tuple-element.185) | copy-start | bytes 7684
  116.3 12.8 %copy-start.56 = (bf16[1,2,4]{2,1,0:T(2,128)(2,1)S(1)}, bf16[1,2,4]{2,1,0:T(2,128)(2,1)}, u32[]{:S(2)}) copy-start(bf16[1,2,4]{2,1,0:T(2,128)(2,1)} %convert_element_type.248) | copy-start | bytes 52
  144.2 16.0 %copy-start.31 = (f32[768]{0:T(1024)S(1)}, f32[768]{0:T(1024)}, u32[]{:S(2)}) copy-start(f32[768]{0:T(1024)} %get-tuple-element.178) | copy-start | bytes 9220
  144.2 16.0 %copy-start.32 = (f32[768]{0:T(1024)S(1)}, f32[768]{0:T(1024)}, u32[]{:S(2)}) copy-start(f32[768]{0:T(1024)} %get-tuple-element.179) | copy-start | bytes 9220
  144.2 16.0 %copy-start.33 = (f32[768]{0:T(1024)S(1)}, f32[768]{0:T(1024)}, u32[]{:S(2)}) copy-start(f32[768]{0:T(1024)} %get-tuple-element.180) | copy-start | bytes 9220
  144.2 16.0 %copy-start.34 = (f32[768]{0:T(1024)S(1)}, f32[768]{0:T(1024)}, u32[]{:S(2)}) copy-start(f32[768]{0:T(1024)} %get-tuple-element.181) | copy-start | bytes 9220
  162.1 18.8 %copy-start.20 = (bf16[128,128]{0,1:T(8,128)(2,1)}, bf16[128,128]{0,1:T(8,128)(2,1)S(1)}, u32[]{:S(2)}) copy-start(bf16[128,128]{0,1:T(8,128)(2,1)S(1)} %copy.166) | copy-start | bytes 98308
  181.5 25.4 %copy-start.3 = (f32[2,4,64,64]{3,2,1,0:T(8,128)}, f32[2,4,64,64]{3,2,1,0:T(8,128)S(1)}, u32[]{:S(2)}) copy-start(f32[2,4,64,64]{3,2,1,0:T(8,128)S(1)} %get-tuple-element.175) | copy-start | bytes 393220
  223.3 8.4 %copy-start.4 = (f32[2,4,64,64]{3,2,1,0:T(8,128)S(1)}, f32[2,4,64,64]{3,2,1,0:T(8,128)}, u32[]{:S(2)}) copy-start(f32[2,4,64,64]{3,2,1,0:T(8,128)} %copy-done.3) | copy-start | bytes 393220
  234.5 9.5 %copy-start.7 = (bf16[64,2048]{1,0:T(8,128)(2,1)S(1)}, bf16[64,2048]{1,0:T(8,128)(2,1)}, u32[]{:S(2)}) copy-start(bf16[64,2048]{1,0:T(8,128)(2,1)} %param.22) | copy-start | bytes 786436
  234.9 9.1 %copy-start.30 = (f32[1,2048]{1,0:T(1,128)S(1)}, f32[1,2048]{1,0:T(1,128)}, u32[]{:S(2)}) copy-start(f32[1,2048]{1,0:T(1,128)} %get-tuple-element.226) | copy-start | bytes 24580
  (35 other events, 123.8 us)
where the time goes:
time: 250 us; the launch traced here: 248 us
  blocking collectives  122 us (49%)
  local copies, waits for them, and re-layouts  58.6 us (23%)
  other arithmetic  34.5 us (14%)
  matrix products  28.4 us (11%)
  starting transfers between devices  3.15 us (1%)
    all_gather x4, blocking collectives, prefix(): lax.all_gather(a.astype(kind), axis)  54.2 us
    psum x1, blocking collectives, local(): lax.psum(jnp.dot(own_cols, modulation, preferred_element_type=jnp.float32...  39.4 us
    all_gather x1, blocking collectives, local(): context_cols = lax.all_gather(own_context, 'sp', axis=0, tiled=True)  14.5 us
    dot_general x10, matrix products, project_many(): jnp.dot(row_block, weight, preferred_element_type=jnp.float32)  10.5 us
    all_gather x1, blocking collectives, local(): lax.all_gather(hidden, 'tp', axis=0, tiled=True)  7.17 us
    all_to_all x1, blocking collectives, local(): lax.all_to_all(stacked, 'tp', split_axis=0, concat_axis=2, tiled=True)[0]  6.85 us
    another operation x3, other arithmetic  6.56 us
    exp x4, local copies, waits for them, and re-layouts, directed_pass(): jnp.exp(running)  5.96 us
  transfers between devices with their start and end apart: 2, of which 0 were waited for; matrix products, arithmetic and copies ran while one was open for 28% of the time, Pallas kernels for 0%

commit v1 on v0

--- a/solution.py
+++ b/solution.py
@@ -207,7 +207,7 @@
         cond_rows, lax.axis_index(("sp", "tp")) * mod_share, mod_share, 1
     )
     mod_rows = lax.psum(
-        jnp.dot(own_cols, modulation, preferred_element_type=jnp.float32), ("sp", "tp")
+        lax.psum(jnp.dot(own_cols, modulation, preferred_element_type=jnp.float32), "tp"), "sp"
     )
     shift_rows = mod_rows[:, :model_width]
     scale_rows = mod_rows[:, model_width : 2 * model_width]

time: 250 us -> 241 us (0.964)
  blocking collectives: 122 us -> 112 us
    psum x1, blocking collectives: 39.4 us -> 10.3 us  [local(): lax.psum(jnp.dot(own_cols, modulation, preferred_element_type=jnp.float32...]
    psum x0 -> x1, blocking collectives: none -> 19.5 us  [local(): lax.psum(lax.psum(jnp.dot(own_cols, modulation, preferred_element_type=jn...]
  transfers between devices with their start and end apart: 2 -> 2, of which waited for: 0 -> 0; matrix products, arithmetic and copies ran while one was open for 28% -> 29% of each run, Pallas kernels for 0% -> 0%
where the time goes in v1:
time: 241 us; the launch traced here: 238 us
  blocking collectives  112 us (46%)
  local copies, waits for them, and re-layouts  58.5 us (24%)
  other arithmetic  34.5 us (14%)
  matrix products  28.4 us (12%)
  starting transfers between devices  3.13 us (1%)
    all_gather x4, blocking collectives, prefix(): lax.all_gather(a.astype(kind), axis)  53.3 us
    psum x1, blocking collectives, local(): lax.psum(lax.psum(jnp.dot(own_cols, modulation, preferred_element_type=jn...  19.5 us
    all_gather x1, blocking collectives, local(): context_cols = lax.all_gather(own_context, 'sp', axis=0, tiled=True)  15.4 us
    dot_general x10, matrix products, project_many(): jnp.dot(row_block, weight, preferred_element_type=jnp.float32)  10.5 us
    psum x1, blocking collectives, local(): lax.psum(jnp.dot(own_cols, modulation, preferred_element_type=jnp.float32...  10.3 us
    all_gather x1, blocking collectives, local(): lax.all_gather(hidden, 'tp', axis=0, tiled=True)  7.17 us
    all_to_all x1, blocking collectives, local(): lax.all_to_all(stacked, 'tp', split_axis=0, concat_axis=2, tiled=True)[0]  6.85 us
    another operation x3, other arithmetic  6.54 us
  transfers between devices with their start and end apart: 2, of which 0 were waited for; matrix products, arithmetic and copies ran while one was open for 29% of the time, Pallas kernels for 0%

profile of v1, /device:TPU:0, one launch (start us, length us, event | category | flops | bytes accessed | tf_op | source)
XLA Modules:
  0.0 238.1 jit_solution(14406622085925360747)
XLA Ops:
  2.4 10.3 %psum.14 = f32[2,6144]{1,0:T(2,128)S(1)} all-reduce(f32[2,6144]{1,0:T(2,128)S(1)} %fusion.93), channel_id=1, replica_groups=mesh['sp'=4,'tp'=2,'dp'=4] {'tp'}, use_global_device_ids=true, to_apply=%region_0.1 | all-reduce | flops 12288 | bytes 98304 | tf_op jit(solution)/shard_map/psum | solution.py:210
  12.7 19.5 %psum.15 = f32[2,6144]{1,0:T(2,128)S(1)} all-reduce(f32[2,6144]{1,0:T(2,128)S(1)} %psum.14), channel_id=1, replica_groups=mesh['sp'=4,'tp'=2,'dp'=4] {'sp'}, use_global_device_ids=true, to_apply=%region_1.2 | all-reduce | flops 12288 | bytes 98304 | tf_op jit(solution)/shard_map/psum | solution.py:209
  33.2 7.2 %all_gather.26 = bf16[128,2048]{1,0:T(8,128)(2,1)S(1)} all-gather(bf16[64,2048]{1,0:T(8,128)(2,1)S(1)} %fusion.31), channel_id=1, replica_groups=mesh['sp'=4,'tp'=2,'dp'=4] {'tp'}, dimensions={0}, use_global_device_ids=true | all-gather | bytes 786432 | tf_op jit(solution)/shard_map/all_gather | solution.py:222
  40.4 2.3 convolution_convert_fusion.2
  43.9 1.9 collective-permute-start
  51.0 2.9 %convolution_convert_fusion.1 = bf16[128,512]{0,1:T(8,128)(2,1)S(1)} fusion(bf16[2048,512]{1,0:T(8,128)(2,1)} %param.28, bf16[128,2048]{1,0:T(8,128)(2,1)} %param.24, f32[2048]{0:T(1024)} %bitcast.249, f32[2048]{0:T(1024)} %bitcast.253, f32[2048]{0:T(1024)S(1)} %convert_element_type.221, f32[128]{0:T(128)S(1)} %add_rsqrt_fusion.1), kind=kOutput, calls=%fused_computation.49 | convolution fusion | flops 270073856 | bytes 2777600 | tf_op jit(solution)/shard_map/dot_general | solution.py:63
  55.6 15.4 %all_gather.30 = bf16[512,656]{0,1:T(8,128)(2,1)S(1)} all-gather(bf16[128,656]{0,1:T(8,128)(2,1)S(1)} %pad_maximum_fusion), channel_id=1, replica_groups=mesh['sp'=4,'tp'=2,'dp'=4] {'sp'}, dimensions={0}, use_global_device_ids=true | all-gather | bytes 839680 | tf_op jit(solution)/shard_map/all_gather | solution.py:243
  84.9 5.0 %reduce-window.6 = f32[2,8,4,128]{3,1,2,0:T(8,128)} reduce-window(f32[2,8,4,128]{3,1,2,0:T(8,128)} %fusion.148, f32[]{:T(128)} %constant.128.clone.1), window={size=1x1x1x128 pad=0_0x0_0x0_0x127_0}, to_apply=%region_8.9 | reduce-window | flops 1040384 | bytes 65540 | tf_op jit(solution)/shard_map/reduce-window
  94.4 2.7 %pad_convert_fusion = f32[515,640]{0,1:T(8,128)} fusion(bf16[512,640]{0,1:T(8,128)(2,1)} %slice.222), kind=kLoop, calls=%fused_computation.67 | loop fusion | flops 329600 | bytes 1973760 | tf_op jit(solution)/shard_map/convert_element_type | solution.py:71
  101.4 3.1 %divide_multiply_fusion = f32[128,512]{1,0:T(8,128)} fusion(bf16[128,2048]{1,0:T(8,128)(2,1)} %copy-done.2, bf16[2048,512]{1,0:T(8,128)(2,1)} %param.29), kind=kOutput, calls=%fused_computation.89 | convolution fusion | flops 268828672 | bytes 2883584 | tf_op jit(solution)/shard_map/dot_general | solution.py:63
  107.5 2.4 multiply_convert_fusion
  109.9 9.0 %all_gather.27 = bf16[4,2,4]{2,1,0:T(2,128)(2,1)} all-gather(bf16[1,2,4]{2,1,0:T(2,128)(2,1)S(1)} %copy-done.55), channel_id=1, replica_groups=mesh['sp'=4,'tp'=2,'dp'=4] {'sp'}, dimensions={0}, use_global_device_ids=true | all-gather | bytes 80 | tf_op jit(solution)/shard_map/all_gather | solution.py:19
  118.9 8.4 %all_gather.31 = bf16[4,2,4]{2,1,0:T(2,128)(2,1)} all-gather(bf16[1,2,4]{2,1,0:T(2,128)(2,1)S(1)} %copy-done.56), channel_id=1, replica_groups=mesh['sp'=4,'tp'=2,'dp'=4] {'sp'}, dimensions={0}, use_global_device_ids=true | all-gather | bytes 80 | tf_op jit(solution)/shard_map/all_gather | solution.py:19
  127.2 1.9 slice.230
  146.3 1.8 copy.190
  154.4 15.4 %all-gather = bf16[8,4,64,64]{3,2,1,0:T(8,128)(2,1)} all-gather(bf16[2,4,64,64]{3,2,1,0:T(8,128)(2,1)S(1)} %fusion.17), channel_id=2, replica_groups=mesh['sp'=4,'tp'=2,'dp'=4] {'sp'}, dimensions={0}, use_global_device_ids=true | all-gather | bytes 327680 | tf_op jit(solution)/shard_map/all_gather | solution.py:19
  176.6 20.6 %all-gather.1 = bf16[8,4,64,64]{3,2,1,0:T(8,128)(2,1)} all-gather(bf16[2,4,64,64]{3,2,1,0:T(8,128)(2,1)S(1)} %fusion.18), channel_id=3, replica_groups=mesh['sp'=4,'tp'=2,'dp'=4] {'sp'}, dimensions={0}, use_global_device_ids=true | all-gather | bytes 327680 | tf_op jit(solution)/shard_map/all_gather | solution.py:19
  197.8 7.0 %while.7 = (s32[]{:T(128)}, f32[2,4]{1,0:T(2,128)}, f32[2,4,64,64]{3,2,1,0:T(8,128)S(1)}, s32[]{:T(128)}, bf16[4,2,4]{2,1,0:T(2,128)(2,1)}, /*index=5*/bf16[4,2,...) while((s32[]{:T(128)}, f32[2,4]{1,0:T(2,128)}, f32[2,4,64,64]{3,2,1,0:T(8,128)S(1)}, ...), condition=%wide.region_13.14_spmd, body=%wide.region_12.13_spmd.sunk | while | flops 98326 | bytes 327979 | solution.py:36
  209.2 1.7 copy.181
  211.9 1.7 fusion.15
  215.8 1.8 rev.23
  222.0 1.7 fusion.16
  227.3 6.8 %all_to_all.15 = bf16[2,64,512]{2,1,0:T(8,128)(2,1)S(1)} all-to-all(bf16[2,64,512]{2,1,0:T(8,128)(2,1)S(1)} %copy.199), channel_id=1, replica_groups=mesh['sp'=4,'tp'=2,'dp'=4] {'tp'}, dimensions={0} | all-to-all | bytes 262144 | tf_op jit(solution)/shard_map/all_to_all | solution.py:281
  234.4 3.8 %fusion.1 = bf16[64,2048]{1,0:T(8,128)(2,1)} fusion(bf16[64,1024]{1,0:T(8,128)(2,1)S(1)} %bitcast.213, bf16[1024,2048]{1,0:T(8,128)(2,1)} %param.39, bf16[64,2048]{1,0:T(8,128)(2,1)S(1)} %copy-done.7, f32[2048]{0:T(1024)S(1)} %bitcast.239), kind=kOutput, calls=%fused_computation.10 | convolution fusion | flops 268959744 | bytes 4857856 | tf_op jit(solution)/shard_map/dot_general | solution.py:280
  (239 shorter events, 90.2 us)
Async XLA Ops:
  1.9 30.9 %copy-start.48 = (bf16[2048]{0:T(1024)(128)(2,1)S(1)}, bf16[2048]{0:T(1024)(128)(2,1)}, u32[]{:S(2)}) copy-start(bf16[2048]{0:T(1024)(128)(2,1)} %param.27) | copy-start | bytes 12292
  1.9 30.9 %copy-start.6 = (bf16[64,2048]{1,0:T(8,128)(2,1)S(1)}, bf16[64,2048]{1,0:T(8,128)(2,1)}, u32[]{:S(2)}) copy-start(bf16[64,2048]{1,0:T(8,128)(2,1)} %param.22) | copy-start | bytes 786436
  33.2 9.5 %copy-start.11 = (bf16[2048,128]{1,0:T(8,128)(2,1)S(1)}, bf16[2048,128]{1,0:T(8,128)(2,1)}, u32[]{:S(2)}) copy-start(bf16[2048,128]{1,0:T(8,128)(2,1)} %param.31) | copy-start | bytes 1572868
  40.4 6.9 %copy-start.2 = (bf16[128,2048]{1,0:T(8,128)(2,1)}, bf16[128,2048]{1,0:T(8,128)(2,1)S(1)}, u32[]{:S(2)}) copy-start(bf16[128,2048]{1,0:T(8,128)(2,1)S(1)} %all_gather.26) | copy-start | bytes 1572868
  43.9 105.6 %collective-permute-start = (bf16[2,768]{1,0:T(2,128)(2,1)}, bf16[2,768]{1,0:T(2,128)(2,1)}, u32[]{:S(2)}, u32[]{:S(2)}) collective-permute-start(bf16[2,768]{1,0:T(2,128)(2,1)} %get-tuple-element.220), channel_id=1, source_target_pairs={{0,8},{8,16},{16,24},{1,9},{9,17},{17,25},{2,10},{10,18},{18,26},{... | collective-permute-start | bytes 9224 | tf_op jit(solution)/shard_map/ppermute | solution.py:44
  45.8 103.7 %collective-permute-start.1 = (bf16[2,768]{1,0:T(2,128)(2,1)}, bf16[2,768]{1,0:T(2,128)(2,1)}, u32[]{:S(2)}, u32[]{:S(2)}) collective-permute-start(bf16[2,768]{1,0:T(2,128)(2,1)} %get-tuple-element.221), channel_id=1, source_target_pairs={{8,0},{16,8},{24,16},{9,1},{17,9},{25,17},{10,2},{18,10},{26,18},{... | collective-permute-start | bytes 9224 | tf_op jit(solution)/shard_map/ppermute | solution.py:47
  47.3 30.5 %copy-start.25 = (f32[128,8]{0,1:T(8,128)}, f32[128,8]{0,1:T(8,128)S(1)}, u32[]{:S(2)}) copy-start(f32[128,8]{0,1:T(8,128)S(1)} %compare_select_fusion.3) | copy-start | bytes 12292
  55.1 15.8 %copy-start.37 = (f32[2,8]{1,0:T(2,128)S(1)}, f32[2,8]{1,0:T(2,128)}, u32[]{:S(2)}) copy-start(f32[2,8]{1,0:T(2,128)} %copy-done.36) | copy-start | bytes 196
  55.5 18.5 %copy-start.41 = (f32[128,8]{0,1:T(8,128)S(1)}, f32[128,8]{0,1:T(8,128)}, u32[]{:S(2)}) copy-start(f32[128,8]{0,1:T(8,128)} %get-tuple-element.233) | copy-start | bytes 12292
  55.5 25.7 %copy-start.38 = (f32[128,8]{0,1:T(8,128)S(1)}, f32[128,8]{0,1:T(8,128)}, u32[]{:S(2)}) copy-start(f32[128,8]{0,1:T(8,128)} %get-tuple-element.232) | copy-start | bytes 12292
  101.4 6.1 %copy-start.1 = (f32[515,640]{0,1:T(8,128)S(1)}, f32[515,640]{0,1:T(8,128)}, u32[]{:S(2)}) copy-start(f32[515,640]{0,1:T(8,128)} %pad_convert_fusion) | copy-start | bytes 3955204
  101.4 6.1 %copy-start.42 = (f32[640]{0:T(1024)S(1)}, f32[640]{0:T(1024)}, u32[]{:S(2)}) copy-start(f32[640]{0:T(1024)} %get-tuple-element.183) | copy-start | bytes 7684
  101.4 6.0 %copy-start.43 = (f32[640]{0:T(1024)S(1)}, f32[640]{0:T(1024)}, u32[]{:S(2)}) copy-start(f32[640]{0:T(1024)} %get-tuple-element.184) | copy-start | bytes 7684
  101.4 6.0 %copy-start.44 = (f32[640]{0:T(1024)S(1)}, f32[640]{0:T(1024)}, u32[]{:S(2)}) copy-start(f32[640]{0:T(1024)} %get-tuple-element.185) | copy-start | bytes 7684
  107.5 11.4 %copy-start.56 = (bf16[1,2,4]{2,1,0:T(2,128)(2,1)S(1)}, bf16[1,2,4]{2,1,0:T(2,128)(2,1)}, u32[]{:S(2)}) copy-start(bf16[1,2,4]{2,1,0:T(2,128)(2,1)} %convert_element_type.248) | copy-start | bytes 52
  134.3 16.0 %copy-start.31 = (f32[768]{0:T(1024)S(1)}, f32[768]{0:T(1024)}, u32[]{:S(2)}) copy-start(f32[768]{0:T(1024)} %get-tuple-element.178) | copy-start | bytes 9220
  134.3 16.0 %copy-start.32 = (f32[768]{0:T(1024)S(1)}, f32[768]{0:T(1024)}, u32[]{:S(2)}) copy-start(f32[768]{0:T(1024)} %get-tuple-element.179) | copy-start | bytes 9220
  134.3 16.1 %copy-start.33 = (f32[768]{0:T(1024)S(1)}, f32[768]{0:T(1024)}, u32[]{:S(2)}) copy-start(f32[768]{0:T(1024)} %get-tuple-element.180) | copy-start | bytes 9220
  134.3 16.1 %copy-start.34 = (f32[768]{0:T(1024)S(1)}, f32[768]{0:T(1024)}, u32[]{:S(2)}) copy-start(f32[768]{0:T(1024)} %get-tuple-element.181) | copy-start | bytes 9220
  152.2 17.6 %copy-start.20 = (bf16[128,128]{0,1:T(8,128)(2,1)}, bf16[128,128]{0,1:T(8,128)(2,1)S(1)}, u32[]{:S(2)}) copy-start(bf16[128,128]{0,1:T(8,128)(2,1)S(1)} %copy.166) | copy-start | bytes 98308
  170.4 26.8 %copy-start.3 = (f32[2,4,64,64]{3,2,1,0:T(8,128)}, f32[2,4,64,64]{3,2,1,0:T(8,128)S(1)}, u32[]{:S(2)}) copy-start(f32[2,4,64,64]{3,2,1,0:T(8,128)S(1)} %get-tuple-element.175) | copy-start | bytes 393220
  213.7 8.4 %copy-start.4 = (f32[2,4,64,64]{3,2,1,0:T(8,128)S(1)}, f32[2,4,64,64]{3,2,1,0:T(8,128)}, u32[]{:S(2)}) copy-start(f32[2,4,64,64]{3,2,1,0:T(8,128)} %copy-done.3) | copy-start | bytes 393220
  224.8 9.5 %copy-start.7 = (bf16[64,2048]{1,0:T(8,128)(2,1)S(1)}, bf16[64,2048]{1,0:T(8,128)(2,1)}, u32[]{:S(2)}) copy-start(bf16[64,2048]{1,0:T(8,128)(2,1)} %param.22) | copy-start | bytes 786436
  225.2 9.1 %copy-start.30 = (f32[1,2048]{1,0:T(1,128)S(1)}, f32[1,2048]{1,0:T(1,128)}, u32[]{:S(2)}) copy-start(f32[1,2048]{1,0:T(1,128)} %get-tuple-element.226) | copy-start | bytes 24580
  (35 other events, 123.6 us)
